TPU v7x, 32 devices: a whole 2x2x4 slice. The times are simulated.
32 devices in a mesh: ep: 8 (over z, x), tp: 4 (over y, core).
Axes of the slice: x: 2, y: 2, z: 4, core: 2. Of those that a mesh axis runs over, the one named last changes fastest.
Arguments:
- conv_input: bfloat16 [4096, 2048], P(('ep', 'tp')), may hold values from -6 to 6
- conv_kernel: float32 [31, 2048], replicated, may hold values from -1 to 1
- conv_gain: float32 [2048], replicated, may hold values from 0.1 to 1.9
- out_weight: bfloat16 [2048, 2048], P(None, 'tp'), may hold values from -0.125 to 0.125
- moe_input: bfloat16 [4096, 2048], P(('ep', 'tp')), may hold values from -6 to 6
- moe_gain: float32 [2048], replicated, may hold values from 0.1 to 1.9
- expert_gate: bfloat16 [8, 2048, 2048], P('ep', None, 'tp'), may hold values from -0.125 to 0.125
- expert_up: bfloat16 [8, 2048, 2048], P('ep', None, 'tp'), may hold values from -0.125 to 0.125
- expert_down: bfloat16 [8, 2048, 2048], P('ep', 'tp'), may hold values from -0.125 to 0.125
- shared_gate: bfloat16 [2048, 128], replicated, may hold values from -0.125 to 0.125
- shared_up: bfloat16 [2048, 128], replicated, may hold values from -0.125 to 0.125
- shared_down: bfloat16 [128, 2048], replicated, may hold values from -0.5 to 0.5
- expert_index: int32 [4096, 2], P('ep'), may hold values from 0 to 7, all different within a row; in each aligned block of 128 rows (0 to 127, 128 to 255, ...) at most 48 rows name the same one
- routing_weight: float32 [4096, 2], P(('ep', 'tp')), may hold values from 0.25 to 1.5
Outputs:
- conv_out: bfloat16 [4096, 2048], P('ep', 'tp')
- moe_out: bfloat16 [4096, 2048], P(('ep', 'tp'))
Inputs may be any that keep to these rules, and one draw needn't show every extreme that they name: `expert_index`: each row names 2 different experts. In each aligned block of 128 rows no expert is named by more than 48 of the rows, and in some blocks one expert is named by exactly 48 rows.
All inputs are finite; a program needn't handle non-finite values.
Results may differ from a plain program's by a relative error of at most 0.009.
Values may be sent and summed in bfloat16 or wider, within the bound.
A program may use at most 128 MiB of HBM per device.

v0:
```python
import jax
import jax.numpy as jnp
from jax import lax
from jax.sharding import PartitionSpec as P

NORM_EPS = 1e-05


def passed_along(block, axis, distance):
    devices = range(lax.axis_size(axis))
    route = [(i - distance, i) for i in devices if i - distance in devices]
    return lax.ppermute(block, axis, route)


def layer_scale(row_data, gain_vec):
    values = row_data.astype(jnp.float32)
    center = values - jnp.mean(values, axis=-1, keepdims=True)
    spread = jnp.mean(center * center, axis=-1, keepdims=True)
    return center * lax.rsqrt(spread + NORM_EPS) * gain_vec


def depthwise(padded, kernel, length):
    running = jnp.zeros((length, padded.shape[1]), jnp.float32)
    for offset in range(kernel.shape[0]):
        running = running + padded[offset : offset + length].astype(jnp.float32) * kernel[offset]
    return running


def slot_table(block_index, experts, slot_count):
    onehot = (
        block_index[:, :, None] == jnp.arange(experts, dtype=jnp.int32)[None, None, :]
    ).astype(jnp.int32)
    before = jnp.cumsum(onehot, axis=1) - onehot
    position = jnp.sum(before * onehot, axis=2)
    return block_index * slot_count + position


def fill_slots(row_data, entry_slot, top_count, total_slots):
    block_count = entry_slot.shape[0]
    entries = entry_slot.shape[1]
    block_ids = jnp.arange(block_count, dtype=jnp.int32)[:, None]
    source = jnp.arange(entries, dtype=jnp.int32)[None, :] // top_count
    slot_row = (
        jnp.zeros((block_count, total_slots), jnp.int32).at[block_ids, entry_slot].set(source)
    )
    filled = jnp.zeros((block_count, total_slots), jnp.int32).at[block_ids, entry_slot].set(1)
    picked = row_data[block_ids, slot_row]
    return jnp.where(filled[:, :, None] > 0, picked, jnp.zeros((), row_data.dtype))


def gated(row_data, gate_weight, up_weight):
    gate_proj = jnp.dot(row_data, gate_weight, preferred_element_type=jnp.float32)
    up_proj = jnp.dot(row_data, up_weight, preferred_element_type=jnp.float32)
    return (jax.nn.silu(gate_proj) * up_proj).astype(jnp.bfloat16)


def on_device(
    conv_input,
    conv_kernel,
    conv_gain,
    out_weight,
    moe_input,
    moe_gain,
    expert_gate,
    expert_up,
    expert_down,
    shared_gate,
    shared_up,
    shared_down,
    expert_index,
    routing_weight,
):
    reach = conv_kernel.shape[0] - 1
    length = conv_input.shape[0]
    halo_rows = passed_along(conv_input[length - reach :], ("ep", "tp"), 1)
    padded = jnp.concatenate([halo_rows, conv_input], axis=0)
    mixed_rows = depthwise(padded, conv_kernel, length)
    normed = jax.nn.silu(layer_scale(mixed_rows, conv_gain)).astype(jnp.bfloat16)
    conv_out = jnp.dot(
        lax.all_gather(normed, "tp", axis=0, tiled=True),
        out_weight,
        preferred_element_type=jnp.float32,
    ).astype(jnp.bfloat16)
    tp_parts = lax.axis_size("tp")
    tp_index = lax.axis_index("tp")
    ep_ranks = lax.axis_size("ep")
    tok_count = moe_input.shape[0]
    top_count = routing_weight.shape[1]
    model_width = moe_input.shape[1]
    experts = ep_ranks * expert_gate.shape[0]
    slot_count = 3 * tok_count * top_count // (2 * experts)
    total_slots = experts * slot_count
    normal = layer_scale(moe_input, moe_gain).astype(jnp.bfloat16)
    group_slots = slot_table(
        expert_index.reshape(tp_parts, tok_count * top_count), experts, slot_count
    )
    own_slots = lax.dynamic_index_in_dim(group_slots, tp_index, 0, keepdims=True)
    gate_local = expert_gate[0]
    up_local = expert_up[0]
    down_local = expert_down[0]
    own_rows = fill_slots(normal[None], own_slots, top_count, total_slots)
    own_rows = own_rows.reshape(ep_ranks, slot_count, model_width)
    arrived = lax.all_to_all(own_rows, "ep", split_axis=0, concat_axis=0, tiled=True)
    hidden = gated(
        lax.all_gather(
            arrived.reshape(ep_ranks * slot_count, model_width), "tp", axis=0, tiled=True
        ),
        gate_local,
        up_local,
    )
    summed = lax.psum_scatter(
        jnp.dot(hidden, down_local, preferred_element_type=jnp.float32).astype(jnp.bfloat16),
        "tp",
        scatter_dimension=0,
        tiled=True,
    )
    returned = lax.all_to_all(
        summed.reshape(ep_ranks, slot_count, model_width),
        "ep",
        split_axis=0,
        concat_axis=0,
        tiled=True,
    )
    picked = returned.reshape(total_slots, model_width)[own_slots[0]]
    picked = picked.reshape(tok_count, top_count, model_width).astype(jnp.float32)
    routed = jnp.sum(picked * routing_weight[:, :, None], axis=1)
    shared_hidden = gated(normal, shared_gate, shared_up)
    shared_part = jnp.dot(shared_hidden, shared_down, preferred_element_type=jnp.float32)
    moe_out = (shared_part + routed).astype(jnp.bfloat16)
    return (conv_out, moe_out)


def solution(mesh):
    in_specs = (
        P(("ep", "tp"), None),
        P(),
        P(),
        P(None, "tp"),
        P(("ep", "tp"), None),
        P(),
        P("ep", None, "tp"),
        P("ep", None, "tp"),
        P("ep", "tp", None),
        P(),
        P(),
        P(),
        P("ep", None),
        P(("ep", "tp"), None),
    )
    out_specs = (P("ep", "tp"), P(("ep", "tp"), None))
    return jax.shard_map(
        on_device, mesh=mesh, in_specs=in_specs, out_specs=out_specs, check_vma=False
    )
```

profile of v0, /device:TPU:0, one launch (start us, length us, event | category | flops | bytes accessed | tf_op | source)
XLA Modules:
  0.0 263.2 jit_solution(7928560640313973617)
XLA Ops:
  7.2 0.0 copy-start
  7.2 0.0 copy-start.1
  7.2 0.0 copy-start.5
  7.2 0.0 all-gather.5.cloned.1.call-start
  7.2 1.0 copy.19
  8.2 0.2 eq.26
  8.4 0.2 reshape.165
  8.6 2.3 reduce-window.6
  10.9 0.1 slice.322
  11.0 0.1 copy.21
  11.1 0.1 fusion.49
  11.3 1.4 scatter_custom_fusion.1
  12.7 1.2 convert_reduce_fusion
  13.9 1.3 fusion.9
  15.3 1.4 scatter_custom_fusion
  16.7 0.1 gt.12
  16.8 0.0 copy-done.1
  16.8 0.0 copy-done.5
  16.8 0.4 fusion.66
  17.2 9.4 %gather_fusion = bf16[384,2048]{1,0:T(8,128)(2,1)} fusion(bf16[1,128,2048]{2,1,0:T(8,128)(2,1)S(1)} %fusion.66, s32[384]{0:T(512)S(1)} %fusion.58), kind=kCustom, calls=%fused_computation | custom fusion | bytes 3148800 | tf_op jit(solution)/shard_map/gather | solution.py:47
  26.6 1.6 broadcast_select_fusion
  28.2 44.2 %all_to_all.10 = bf16[8,48,2048]{2,1,0:T(8,128)(2,1)} all-to-all(bf16[8,48,2048]{2,1,0:T(8,128)(2,1)S(1)} %broadcast_select_fusion), channel_id=1, replica_groups=mesh['ep'=8,'tp'=4] {'ep'}, dimensions={0} | all-to-all | bytes 3145728 | tf_op jit(solution)/shard_map/all_to_all | solution.py:103
  72.3 0.0 all-gather.5.cloned.1.call-update
  72.4 0.2 reduce-scatter.2.cloned.1.call-start
  72.6 45.3 %all-gather.5.cloned.1.call-done = bf16[1536,2048]{1,0:T(8,128)(2,1)} async-done(((bf16[384,2048]{1,0:T(8,128)(2,1)}), bf16[1536,2048]{1,0:T(8,128)(2,1)}) %all-gather.5.cloned.1.call-update) | async-done | bytes 6291472 | tf_op jit(solution)/shard_map/all_gather | solution.py:105
  117.9 8.5 %fusion.4 = f32[1536,512]{1,0:T(8,128)} fusion(bf16[1536,2048]{1,0:T(8,128)(2,1)} %all-gather.5.cloned.1.call-done, bf16[1,2048,512]{2,1,0:T(8,128)(2,1)} %param.20), kind=kOutput, calls=%fused_computation.40 | convolution fusion | flops 3221225472 | bytes 11534336 | tf_op jit(solution)/shard_map/dot_general | solution.py:52
  126.4 0.0 copy-done
  126.4 11.8 %convolution_convert_fusion = bf16[1536,2048]{1,0:T(8,128)(2,1)} fusion(bf16[1,512,2048]{2,1,0:T(8,128)(2,1)S(1)} %copy-done, bf16[1536,2048]{1,0:T(8,128)(2,1)} %all-gather.5.cloned.1.call-done, f32[1536,512]{1,0:T(8,128)} %fusion.4, bf16[1,2048,512]{2,1,0:T(8,128)(2,1)} %param.21), kind=kOutput, calls=%fused_computation.4 | convolution fusion | flops 6450315264 | bytes 19922944 | tf_op jit(solution)/shard_map/dot_general | solution.py:112
  138.2 0.0 copy-start.2
  138.2 0.0 copy-start.4
  138.2 0.0 reduce-scatter.2.cloned.1.call-update
  138.3 0.0 copy-start.6
  138.3 0.0 all-gather.3.cloned.1.call-start
  138.3 1.0 copy-done.2
  139.3 2.2 collective-permute-start
  141.5 0.0 copy-done.4
  141.5 0.1 fusion.72
  141.6 0.1 fusion.73
  141.7 0.8 collective-permute-done
  142.5 4.8 %fusion.71 = (f32[128]{0:T(128)S(1)}, f32[128,2048]{1,0:T(8,128)S(1)}) fusion(f32[2048]{0:T(1024)S(1)} %bitcast.111, bf16[128,2048]{1,0:T(8,128)(2,1)S(1)} %copy-done.2, f32[2048]{0:T(1024)S(1)} %bitcast.112, bf16[30,2048]{1,0:T(8,128)(2,1)S(1)} %collective-permute-done, f32[2048]{0:T(1024)S(1)} %bitcast.83, f32[2048]{0:T(1024)S(1)} %bitcast.84, ...), kind=kLoop, calls=%fused_computation.162 | loop fusion | flops 47972224 | bytes 1950208 | tf_op jit(solution)/shard_map/reduce_sum | solution.py:17
  147.3 0.3 multiply_reduce_fusion.1
  147.6 0.0 copy-done.6
  147.6 1.2 multiply_convert_fusion
  148.8 0.0 copy-start.7
  148.8 0.0 copy-start.8
  148.8 0.0 all-gather.3.cloned.1.call-update
  148.8 48.4 %reduce-scatter.2.cloned.1.call-done = bf16[384,2048]{1,0:T(8,128)(2,1)} async-done(((bf16[1536,2048]{1,0:T(8,128)(2,1)}), bf16[384,2048]{1,0:T(8,128)(2,1)}) %reduce-scatter.2.cloned.1.call-update) | async-done | bytes 1572880 | tf_op jit(solution)/shard_map/reduce_scatter | solution.py:111
  197.3 5.5 %all-to-all-start.1 = ((bf16[8,48,2048]{2,1,0:T(8,128)(2,1)}), bf16[8,48,2048]{2,1,0:T(8,128)(2,1)}, u32[]{:S(2)}, u32[]{:S(2)}) async-start(bf16[8,48,2048]{2,1,0:T(8,128)(2,1)} %bitcast.81), calls=%async_computation.2 | async-start | bytes 3145728 | tf_op jit(solution)/shard_map/all_to_all | solution.py:117
  202.8 0.0 copy-done.7
  202.8 0.1 copy.23
  202.9 0.0 copy-done.8
  202.9 0.4 fusion.69
  203.3 18.7 %all-gather.3.cloned.1.call-done = bf16[512,2048]{1,0:T(8,128)(2,1)} async-done(((bf16[128,2048]{1,0:T(8,128)(2,1)}), bf16[512,2048]{1,0:T(8,128)(2,1)}) %all-gather.3.cloned.1.call-update) | async-done | bytes 2097168 | tf_op jit(solution)/shard_map/all_gather | solution.py:80
  222.0 4.3 %convolution_convert_fusion.1 = bf16[512,512]{1,0:T(8,128)(2,1)} fusion(bf16[512,2048]{1,0:T(8,128)(2,1)} %all-gather.3.cloned.1.call-done, bf16[2048,512]{1,0:T(8,128)(2,1)} %param.17), kind=kOutput, calls=%fused_computation.46 | convolution fusion | flops 1074003968 | bytes 4718592 | tf_op jit(solution)/shard_map/dot_general | solution.py:79
  226.3 13.5 %all-to-all-done.1 = bf16[8,48,2048]{2,1,0:T(8,128)(2,1)} async-done(((bf16[8,48,2048]{2,1,0:T(8,128)(2,1)}), bf16[8,48,2048]{2,1,0:T(8,128)(2,1)}, u32[]{:S(2)}, u32[]{:S(2)}) %all-to-all-start.1) | async-done | bytes 1572896 | tf_op jit(solution)/shard_map/all_to_all | solution.py:117
  239.7 5.0 %gather_fusion.1 = bf16[256,2048]{1,0:T(8,128)(2,1)} fusion(bf16[384,2048]{1,0:T(8,128)(2,1)} %bitcast.47, s32[1024]{0:T(1024)S(1)} %pad_clamp_fusion), kind=kCustom, calls=%fused_computation.1 | custom fusion | bytes 2098176 | tf_op jit(solution)/shard_map/gather | solution.py:124
  244.7 3.4 %reshape.170 = f32[128,2,2048]{2,1,0:T(2,128)} reshape(bf16[256,2048]{1,0:T(8,128)(2,1)} %gather_fusion.1) | data formatting | bytes 3145728 | tf_op jit(solution)/shard_map/convert_element_type | solution.py:125
  248.1 0.0 copy-start.3
  248.1 5.8 %multiply_reduce_fusion = f32[128,2048]{1,0:T(8,128)} fusion(f32[128,2,2048]{2,1,0:T(2,128)} %reshape.170, f32[128,2]{1,0:T(8,128)S(1)} %copy.23), kind=kLoop, calls=%fused_computation.42 | loop fusion | flops 786432 | bytes 3146752 | tf_op jit(solution)/shard_map/reduce_sum | solution.py:126
  253.9 0.0 copy-done.3
  253.9 2.8 %fusion.1 = bf16[128,2048]{1,0:T(8,128)(2,1)} fusion(f32[128,2048]{1,0:T(8,128)} %multiply_reduce_fusion, bf16[128,2048]{1,0:T(8,128)(2,1)S(1)} %copy-done.3, bf16[2048,128]{1,0:T(8,128)(2,1)} %param.24, f32[128,128]{1,0:T(8,128)S(1)} %fusion.69, bf16[128,2048]{1,0:T(8,128)(2,1)S(1)} %copy-done.1, f32[2048]{0:T(1024)S(1)} %copy-done.5, ...), kind=kOutput, calls=%fused_computation.37 | convolution fusion | flops 136151040 | bytes 3220480 | tf_op jit(solution)/shard_map/dot_general | solution.py:128
  (20 shorter events, 0.2 us)
Async XLA Ops:
  7.2 119.3 %copy-start = (bf16[1,512,2048]{2,1,0:T(8,128)(2,1)S(1)}, bf16[1,512,2048]{2,1,0:T(8,128)(2,1)}, u32[]{:S(2)}) copy-start(bf16[1,512,2048]{2,1,0:T(8,128)(2,1)} %param.22) | copy-start | bytes 6291460
  7.2 9.6 %copy-start.1 = (bf16[128,2048]{1,0:T(8,128)(2,1)S(1)}, bf16[128,2048]{1,0:T(8,128)(2,1)}, u32[]{:S(2)}) copy-start(bf16[128,2048]{1,0:T(8,128)(2,1)} %param.18) | copy-start | bytes 1572868
  7.2 9.6 %copy-start.5 = (f32[2048]{0:T(1024)S(1)}, f32[2048]{0:T(1024)}, u32[]{:S(2)}) copy-start(f32[2048]{0:T(1024)} %param.19) | copy-start | bytes 24580
  7.2 110.7 %all-gather.5.cloned.1.call-start = ((), (), s32[]{:S(2)}) async-start(), calls=%async_computation.4 | async-start | bytes 7864320 | tf_op jit(solution)/shard_map/all_gather | solution.py:105
  72.4 124.9 %reduce-scatter.2.cloned.1.call-start = ((), (), s32[]{:S(2)}) async-start(), calls=%async_computation.5 | async-start | bytes 7864320 | tf_op jit(solution)/shard_map/reduce_scatter | solution.py:111
  138.2 1.0 copy-start.2
  138.2 3.3 %copy-start.4 = (f32[31,2048]{1,0:T(8,128)S(1)}, f32[31,2048]{1,0:T(8,128)}, u32[]{:S(2)}) copy-start(f32[31,2048]{1,0:T(8,128)} %param.15) | copy-start | bytes 761860
  138.3 9.3 %copy-start.6 = (f32[2048]{0:T(1024)S(1)}, f32[2048]{0:T(1024)}, u32[]{:S(2)}) copy-start(f32[2048]{0:T(1024)} %param.16) | copy-start | bytes 24580
  138.3 83.8 %all-gather.3.cloned.1.call-start = ((), (), s32[]{:S(2)}) async-start(), calls=%async_computation.3 | async-start | bytes 2621440 | tf_op jit(solution)/shard_map/all_gather | solution.py:80
  139.3 3.2 %collective-permute-start = (bf16[30,2048]{1,0:T(8,128)(2,1)S(1)}, bf16[30,2048]{1,0:T(8,128)(2,1)S(1)}, u32[]{:S(2)}, u32[]{:S(2)}) collective-permute-start(bf16[30,2048]{1,0:T(8,128)(2,1)S(1)} %slice.192), channel_id=1, source_target_pairs={{0,1},{1,2},{2,3},{3,4},{4,5},{5,6},{6,7},{7,8},{8,9},{9,10},{10,1... | collective-permute-start | bytes 368648 | tf_op jit(solution)/shard_map/ppermute | solution.py:12
  148.8 54.0 %copy-start.7 = (f32[128,2]{0,1:T(2,128)S(1)}, f32[128,2]{0,1:T(2,128)}, u32[]{:S(2)}) copy-start(f32[128,2]{0,1:T(2,128)} %param.27) | copy-start | bytes 3076
  148.8 54.1 %copy-start.8 = (bf16[2048,128]{1,0:T(8,128)(2,1)S(1)}, bf16[2048,128]{1,0:T(8,128)(2,1)}, u32[]{:S(2)}) copy-start(bf16[2048,128]{1,0:T(8,128)(2,1)} %param.23) | copy-start | bytes 1572868
  197.3 42.5 %all-to-all-start.1 = ((bf16[8,48,2048]{2,1,0:T(8,128)(2,1)}), bf16[8,48,2048]{2,1,0:T(8,128)(2,1)}, u32[]{:S(2)}, u32[]{:S(2)}) async-start(bf16[8,48,2048]{2,1,0:T(8,128)(2,1)} %bitcast.81), calls=%async_computation.2 | async-start | bytes 3145728 | tf_op jit(solution)/shard_map/all_to_all | solution.py:117
  248.1 5.8 %copy-start.3 = (bf16[128,2048]{1,0:T(8,128)(2,1)S(1)}, bf16[128,2048]{1,0:T(8,128)(2,1)}, u32[]{:S(2)}) copy-start(bf16[128,2048]{1,0:T(8,128)(2,1)} %param.25) | copy-start | bytes 1572868
Sparse Core Ops, SparseCore 0:
  72.5 45.3 all-gather.4
  138.4 58.8 reduce-scatter.1
  199.4 22.5 all-gather.2
where the time goes:
time: 264 us; the launch traced here: 263 us
  waiting for transfers between devices  127 us (48%)
  blocking collectives  44.2 us (17%)
  matrix products  27.7 us (10%)
  local copies, waits for them, and re-layouts  23.5 us (9%)
  other arithmetic  19 us (7%)
  between operations  14 us (5%)
  starting transfers between devices  8 us (3%)
    reduce_scatter x1, waiting for transfers between devices, on_device(): lax.psum_scatter(jnp.dot(hidden, down_local, preferred_element_type=jnp.f...  48.4 us
    all_gather x1, waiting for transfers between devices, on_device(): lax.all_gather(arrived.reshape(ep_ranks * slot_count, model_width), 'tp',...  45.3 us
    all_to_all x1, blocking collectives, on_device(): lax.all_to_all(own_rows, 'ep', split_axis=0, concat_axis=0, tiled=True)  44.2 us
    all_gather x1, waiting for transfers between devices, on_device(): lax.all_gather(normed, 'tp', axis=0, tiled=True)  18.7 us
    all_to_all x1, waiting for transfers between devices, on_device(): lax.all_to_all(summed.reshape(ep_ranks, slot_count, model_width), 'ep', s...  13.5 us
    dot_general x1, matrix products, on_device(): jnp.dot(hidden, down_local, preferred_element_type=jnp.float32)  11.8 us
    gather x1, local copies, waits for them, and re-layouts, fill_slots(): picked = row_data[block_ids, slot_row]  9.42 us
    dot_general x2, matrix products, gated(): jnp.dot(row_data, gate_weight, preferred_element_type=jnp.float32)  8.89 us
  transfers between devices with their start and end apart: 5, of which 5 were waited for; matrix products, arithmetic and copies ran while one was open for 4% of the time, Pallas kernels for 0%

commit v1 on v0

--- a/solution.py
+++ b/solution.py
@@ -1,6 +1,10 @@
+import functools
+
 import jax
 import jax.numpy as jnp
 from jax import lax
+from jax.experimental import pallas as pl
+from jax.experimental.pallas import tpu as pltpu
 from jax.sharding import PartitionSpec as P
 
 NORM_EPS = 1e-05
@@ -130,6 +134,429 @@
     return (conv_out, moe_out)
 
 
+LANES = 128
+ROW_TILE = 16
+COLS = 512
+MESH = pl.DeviceIdType.MESH
+
+
+def fused_kernel(
+    n,
+    slots,
+    reach,
+    conv_in,
+    taps,
+    conv_gain,
+    out_w_hbm,
+    moe_in,
+    moe_gain,
+    gate_hbm,
+    up_hbm,
+    down_hbm,
+    sh_gate,
+    sh_up,
+    sh_down,
+    index_ref,
+    weight_ref,
+    conv_out,
+    moe_out,
+    own,
+    gath,
+    part,
+    from_core,
+    pair_sum,
+    from_y,
+    result,
+    returned,
+    normal,
+    halo,
+    pad,
+    mixed,
+    conv_all,
+    gate_w,
+    up_w,
+    down_w,
+    out_w,
+    local_sem,
+    chunk_send,
+    chunk_recv,
+    conv_send,
+    conv_recv,
+):
+    tokens, width = moe_in.shape
+    e = lax.axis_index("ep")
+    t = lax.axis_index("tp")
+    core = lax.rem(t, 2)
+    row = t // 2
+    core_peer = row * 2 + (1 - core)
+    y_peer = (1 - row) * 2 + core
+    diagonal = (1 - row) * 2 + (1 - core)
+    place = e * 4 + t
+    after = lax.rem(place + 1, n * 4)
+    ahead = lax.rem(place + n * 4 - 1, n * 4)
+    halo_rows = halo.shape[0]
+
+    fetches = [
+        pltpu.make_async_copy(src, dst, local_sem.at[i])
+        for i, (src, dst) in enumerate(
+            ((gate_hbm.at[0], gate_w), (up_hbm.at[0], up_w), (down_hbm.at[0], down_w), (out_w_hbm, out_w))
+        )
+    ]
+    for fetch in fetches:
+        fetch.start()
+
+    barrier = pltpu.get_barrier_semaphore()
+    greeted = [(lax.rem(e + k, n), t) for k in range(1, n)]
+    greeted += [(e, core_peer), (e, y_peer)]
+    greeted += [(after // 4, lax.rem(after, 4)), (ahead // 4, lax.rem(ahead, 4))]
+    for device in greeted:
+        pl.semaphore_signal(barrier, inc=1, device_id=device, device_id_type=MESH)
+    pl.semaphore_wait(barrier, len(greeted))
+
+    def remote(src, dst, kind, k, device):
+        return pltpu.make_async_remote_copy(
+            src_ref=src,
+            dst_ref=dst,
+            send_sem=chunk_send.at[kind, k],
+            recv_sem=chunk_recv.at[kind, k],
+            device_id=device,
+            device_id_type=MESH,
+        )
+
+    def conv_copy(src, dst, kind, device):
+        return pltpu.make_async_remote_copy(
+            src_ref=src,
+            dst_ref=dst,
+            send_sem=conv_send.at[kind],
+            recv_sem=conv_recv.at[kind],
+            device_id=device,
+            device_id_type=MESH,
+        )
+
+    def dispatch_copy(k):
+        return remote(own.at[k], gath.at[k, t], 0, k, (lax.rem(e + k, n), t))
+
+    def share_core(k, q):
+        return remote(gath.at[k, q], gath.at[k, q], 1, k, (e, core_peer))
+
+    def share_y(k, q):
+        return remote(gath.at[k, q], gath.at[k, q], 2, k, (e, y_peer))
+
+    def forward_core(k, q):
+        return remote(gath.at[k, q], gath.at[k, q], 3, k, (e, core_peer))
+
+    def reduce_core(k, q, which):
+        return remote(part.at[k, q], from_core.at[which, k], 4 + which, k, (e, core_peer))
+
+    def reduce_y(k):
+        return remote(pair_sum.at[k], from_y.at[k], 6, k, (e, y_peer))
+
+    def return_copy(k):
+        return remote(result.at[k], returned.at[k], 7, k, (lax.rem(e - k + n, n), t))
+
+    halo_copy = conv_copy(
+        conv_in.at[pl.ds(tokens - halo_rows, halo_rows)],
+        halo,
+        0,
+        (after // 4, lax.rem(after, 4)),
+    )
+    halo_copy.start()
+
+    def normal_rows(i, carry):
+        rows = pl.ds(pl.multiple_of(i * ROW_TILE, ROW_TILE), ROW_TILE)
+        normal[rows, :] = layer_scale(moe_in[rows, :], moe_gain[...]).astype(jnp.bfloat16)
+        return carry
+
+    lax.fori_loop(0, tokens // ROW_TILE, normal_rows, 0)
+
+    chosen = index_ref[pl.ds(pl.multiple_of(t * tokens, tokens), tokens), :]
+    relative = chosen - e
+    relative = jnp.where(relative < 0, relative + n, relative)
+    first, second = relative[:, 0:1], relative[:, 1:2]
+    lane = lax.broadcasted_iota(jnp.int32, (tokens, LANES), 1)
+    hot_first = (lane == first).astype(jnp.float32)
+    hot_second = (lane == second).astype(jnp.float32)
+    earlier = (
+        lax.broadcasted_iota(jnp.int32, (tokens, tokens), 0)
+        > lax.broadcasted_iota(jnp.int32, (tokens, tokens), 1)
+    ).astype(jnp.float32).astype(jnp.bfloat16)
+    before = jnp.dot(
+        earlier, (hot_first + hot_second).astype(jnp.bfloat16), preferred_element_type=jnp.float32
+    )
+    slot_first = first.astype(jnp.float32) * slots + jnp.sum(before * hot_first, axis=1, keepdims=True)
+    slot_second = second.astype(jnp.float32) * slots + jnp.sum(
+        before * hot_second, axis=1, keepdims=True
+    )
+    row_first = jnp.broadcast_to(slot_first, (tokens, LANES)).T[0:1, :]
+    row_second = jnp.broadcast_to(slot_second, (tokens, LANES)).T[0:1, :]
+    slot_row = lax.broadcasted_iota(jnp.int32, (n * slots, tokens), 0).astype(jnp.float32)
+    spread = (
+        jnp.where(slot_row == row_first, 1.0, 0.0) + jnp.where(slot_row == row_second, 1.0, 0.0)
+    ).astype(jnp.bfloat16)
+    for c in range(0, width, COLS):
+        rows = jnp.dot(spread, normal[:, c : c + COLS], preferred_element_type=jnp.float32)
+        rows = rows.astype(jnp.bfloat16).reshape(n, slots, COLS)
+        own[:, :, c : c + COLS] = rows
+        gath[0, t, :, c : c + COLS] = rows[0]
+
+    for k in range(1, n):
+        dispatch_copy(k).start()
+
+    def relay(k):
+        share_y(k, t).start()
+        share_core(k, t).start()
+
+    def forward(k):
+        share_y(k, y_peer).wait_recv()
+        forward_core(k, y_peer).start()
+
+    relay(0)
+
+    conv_copy(halo, halo, 0, (e, core_peer)).wait_recv()
+    inside = jnp.where(place == 0, 0.0, 1.0)
+    pad[0:halo_rows, :] = halo[...].astype(jnp.float32) * inside
+    pad[halo_rows:, :] = conv_in[...].astype(jnp.float32)
+
+    def strip(c, carry):
+        cols = pl.ds(pl.multiple_of(c * LANES, LANES), LANES)
+        total = jnp.zeros((tokens, LANES), jnp.float32)
+        for k in range(reach + 1):
+            start = halo_rows - reach + k
+            total = total + pad[pl.ds(start, tokens), cols] * taps[pl.ds(k, 1), cols]
+        mixed[:, cols] = total
+        return carry
+
+    lax.fori_loop(0, width // LANES, strip, 0)
+
+    def conv_rows(i, carry):
+        rows = pl.ds(pl.multiple_of(i * ROW_TILE, ROW_TILE), ROW_TILE)
+        conv_all[t, rows, :] = jax.nn.silu(layer_scale(mixed[rows, :], conv_gain[...])).astype(
+            jnp.bfloat16
+        )
+        return carry
+
+    lax.fori_loop(0, tokens // ROW_TILE, conv_rows, 0)
+    conv_y = conv_copy(conv_all.at[t], conv_all.at[t], 1, (e, y_peer))
+    conv_core = conv_copy(conv_all.at[t], conv_all.at[t], 2, (e, core_peer))
+    conv_pass = conv_copy(conv_all.at[y_peer], conv_all.at[y_peer], 3, (e, core_peer))
+    conv_y.start()
+    conv_core.start()
+
+    dispatch_copy(1).wait_recv()
+    relay(1)
+    forward(0)
+    for fetch in fetches[:3]:
+        fetch.wait()
+
+    def step(i, carry):
+        @pl.when(i + 2 < n)
+        def _():
+            k = i + 2
+            dispatch_copy(k).wait_recv()
+            relay(k)
+
+        @pl.when(i + 1 < n)
+        def _():
+            forward(i + 1)
+
+        @pl.when(i == 2)
+        def _():
+            conv_copy(conv_all.at[y_peer], conv_all.at[y_peer], 1, (e, y_peer)).wait_recv()
+            conv_pass.start()
+
+        @pl.when(i < n)
+        def _():
+            share_core(i, core_peer).wait_recv()
+            forward_core(i, diagonal).wait_recv()
+            rows = gath[i].reshape(4 * slots, width)
+            hidden = gated(rows, gate_w[...], up_w[...])
+            for c in range(0, width, COLS):
+                piece = jnp.dot(hidden, down_w[:, c : c + COLS], preferred_element_type=jnp.float32)
+                part[i, :, :, c : c + COLS] = piece.astype(jnp.bfloat16).reshape(4, slots, COLS)
+            reduce_core(i, diagonal, 1).start()
+            reduce_core(i, core_peer, 0).start()
+
+        @pl.when((i >= 1) & (i <= n))
+        def _():
+            k = i - 1
+            reduce_core(k, core_peer, 1).wait_recv()
+            pair_sum[k] = (
+                part[k, y_peer].astype(jnp.float32) + from_core[1, k].astype(jnp.float32)
+            ).astype(jnp.bfloat16)
+            reduce_y(k).start()
+
+        @pl.when(i >= 2)
+        def _():
+            k = i - 2
+            reduce_core(k, core_peer, 0).wait_recv()
+            reduce_y(k).wait_recv()
+            total = part[k, t].astype(jnp.float32) + from_core[0, k].astype(jnp.float32)
+            total = (total + from_y[k].astype(jnp.float32)).astype(jnp.bfloat16)
+
+            @pl.when(k > 0)
+            def _():
+                result[k] = total
+                return_copy(k).start()
+
+            @pl.when(k == 0)
+            def _():
+                returned[0] = total
+
+        return carry
+
+    lax.fori_loop(0, n + 2, step, 0)
+
+    conv_copy(conv_all.at[core_peer], conv_all.at[core_peer], 2, (e, core_peer)).wait_recv()
+    conv_copy(conv_all.at[diagonal], conv_all.at[diagonal], 3, (e, core_peer)).wait_recv()
+    fetches[3].wait()
+    for q in range(4):
+        conv_out[q * tokens : (q + 1) * tokens, :] = jnp.dot(
+            conv_all[q], out_w[...], preferred_element_type=jnp.float32
+        ).astype(jnp.bfloat16)
+
+    shared = gated(normal[...], sh_gate[...], sh_up[...])
+    slot_lane = lax.broadcasted_iota(jnp.int32, (tokens, n * slots), 1).astype(jnp.float32)
+    share = jnp.where(slot_lane == slot_first, weight_ref[:, 0:1], 0.0) + jnp.where(
+        slot_lane == slot_second, weight_ref[:, 1:2], 0.0
+    )
+    share_high = share.astype(jnp.bfloat16)
+    share_low = (share - share_high.astype(jnp.float32)).astype(jnp.bfloat16)
+    for k in range(1, n):
+        return_copy(k).wait_recv()
+    for c in range(0, width, COLS):
+        rows = returned[:, :, c : c + COLS].reshape(n * slots, COLS)
+        total = jnp.dot(shared, sh_down[:, c : c + COLS], preferred_element_type=jnp.float32)
+        total = total + jnp.dot(share_high, rows, preferred_element_type=jnp.float32)
+        total = total + jnp.dot(share_low, rows, preferred_element_type=jnp.float32)
+        moe_out[:, c : c + COLS] = total.astype(jnp.bfloat16)
+
+    halo_copy.wait_send()
+    conv_y.wait_send()
+    conv_core.wait_send()
+    conv_pass.wait_send()
+
+    def drain(k, carry):
+        @pl.when(k > 0)
+        def _():
+            dispatch_copy(k).wait_send()
+            return_copy(k).wait_send()
+
+        share_y(k, t).wait_send()
+        share_core(k, t).wait_send()
+        forward_core(k, y_peer).wait_send()
+        reduce_core(k, diagonal, 1).wait_send()
+        reduce_core(k, core_peer, 0).wait_send()
+        reduce_y(k).wait_send()
+        return carry
+
+    lax.fori_loop(0, n, drain, 0)
+
+
+def fused(
+    conv_input,
+    conv_kernel,
+    conv_gain,
+    out_weight,
+    moe_input,
+    moe_gain,
+    expert_gate,
+    expert_up,
+    expert_down,
+    shared_gate,
+    shared_up,
+    shared_down,
+    expert_index,
+    routing_weight,
+):
+    n = lax.axis_size("ep")
+    parts = lax.axis_size("tp")
+    tokens, width = moe_input.shape
+    slots = 3 * tokens * routing_weight.shape[1] // (2 * n)
+    hidden = expert_gate.shape[2]
+    reach = conv_kernel.shape[0] - 1
+    halo_rows = -(-reach // ROW_TILE) * ROW_TILE
+    out_cols = out_weight.shape[1]
+    bf16 = jnp.bfloat16
+    chunk = (n, slots, width)
+    vmem = pl.BlockSpec(memory_space=pltpu.VMEM)
+    hbm = pl.BlockSpec(memory_space=pl.ANY)
+    return pl.pallas_call(
+        functools.partial(fused_kernel, n, slots, reach),
+        out_shape=(
+            jax.ShapeDtypeStruct((parts * tokens, out_cols), bf16),
+            jax.ShapeDtypeStruct((tokens, width), bf16),
+        ),
+        in_specs=[vmem, vmem, vmem, hbm, vmem, vmem, hbm, hbm, hbm, vmem, vmem, vmem, vmem, vmem],
+        out_specs=(vmem, vmem),
+        scratch_shapes=[
+            pltpu.VMEM(chunk, bf16),
+            pltpu.VMEM((n, parts, slots, width), bf16),
+            pltpu.VMEM((n, parts, slots, width), bf16),
+            pltpu.VMEM((2,) + chunk, bf16),
+            pltpu.VMEM(chunk, bf16),
+            pltpu.VMEM(chunk, bf16),
+            pltpu.VMEM(chunk, bf16),
+            pltpu.VMEM(chunk, bf16),
+            pltpu.VMEM((tokens, width), bf16),
+            pltpu.VMEM((halo_rows, width), bf16),
+            pltpu.VMEM((halo_rows + tokens, width), jnp.float32),
+            pltpu.VMEM((tokens, width), jnp.float32),
+            pltpu.VMEM((parts, tokens, width), bf16),
+            pltpu.VMEM((width, hidden), bf16),
+            pltpu.VMEM((width, hidden), bf16),
+            pltpu.VMEM((hidden, width), bf16),
+            pltpu.VMEM((width, out_cols), bf16),
+            pltpu.SemaphoreType.DMA((4,)),
+            pltpu.SemaphoreType.DMA((8, n)),
+            pltpu.SemaphoreType.DMA((8, n)),
+            pltpu.SemaphoreType.DMA((4,)),
+            pltpu.SemaphoreType.DMA((4,)),
+        ],
+        compiler_params=pltpu.CompilerParams(
+            collective_id=0, has_side_effects=True, vmem_limit_bytes=60 * 1024 * 1024
+        ),
+    )(
+        conv_input,
+        conv_kernel,
+        conv_gain.reshape(1, width),
+        out_weight,
+        moe_input,
+        moe_gain.reshape(1, width),
+        expert_gate,
+        expert_up,
+        expert_down,
+        shared_gate,
+        shared_up,
+        shared_down,
+        expert_index,
+        routing_weight,
+    )
+
+
+def fits_fused(args):
+    n, parts = lax.axis_size("ep"), lax.axis_size("tp")
+    conv_input, conv_kernel, moe_input = args[0], args[1], args[4]
+    top_count = args[13].shape[1]
+    tokens, width = moe_input.shape
+    slots = 3 * tokens * top_count // (2 * n)
+    return (
+        parts == 4
+        and top_count == 2
+        and args[6].shape[0] == 1
+        and conv_input.shape == moe_input.shape
+        and conv_kernel.shape[0] - 1 <= tokens
+        and tokens % LANES == 0
+        and width % COLS == 0
+        and slots % ROW_TILE == 0
+        and slots >= ROW_TILE
+        and n <= LANES
+    )
+
+
+def either(*args):
+    return fused(*args) if fits_fused(args) else on_device(*args)
+
+
 def solution(mesh):
     in_specs = (
         P(("ep", "tp"), None),
@@ -149,5 +576,5 @@
     )
     out_specs = (P("ep", "tp"), P(("ep", "tp"), None))
     return jax.shard_map(
-        on_device, mesh=mesh, in_specs=in_specs, out_specs=out_specs, check_vma=False
-    )
+        either, mesh=mesh, in_specs=in_specs, out_specs=out_specs, check_vma=False
+    )

time: 264 us -> 118 us (0.45)
  waiting for transfers between devices: 127 us -> 0 us
  Pallas kernels: 0 us -> 111 us
  blocking collectives: 44.2 us -> 0 us
  matrix products: 27.7 us -> 0 us
  other arithmetic: 19 us -> 0 us
  local copies, waits for them, and re-layouts: 23.5 us -> 6.7 us
  between operations: 14 us -> 0.64 us
  starting transfers between devices: 8 us -> 0 us
    pallas_call x0 -> x1, Pallas kernels: none -> 111 us  [fused(): pl.pallas_call(functools.partial(fused_kernel, n, slots, reach), out_shap...]
    all_gather x2 -> x0, waiting for transfers between devices: 64 us -> none  [the longest x1 45.3 us: on_device(): lax.all_gather(arrived.reshape(ep_ranks * slot_count, model_width), 'tp',...]
    reduce_scatter x1 -> x0, waiting for transfers between devices: 48.4 us -> none  [on_device(): lax.psum_scatter(jnp.dot(hidden, down_local, preferred_element_type=jnp.f...]
    all_to_all x1 -> x0, blocking collectives: 44.2 us -> none  [on_device(): lax.all_to_all(own_rows, 'ep', split_axis=0, concat_axis=0, tiled=True)]
    dot_general x5 -> x0, matrix products: 27.7 us -> none  [the longest x1 11.8 us: on_device(): jnp.dot(hidden, down_local, preferred_element_type=jnp.float32)]
    gather x2 -> x0, local copies, waits for them, and re-layouts: 14.4 us -> none  [the longest x1 9.42 us: fill_slots(): picked = row_data[block_ids, slot_row]]
    reduce_sum x6 -> x0, other arithmetic: 13.5 us -> none  [the longest x2 6.01 us: layer_scale(): center = values - jnp.mean(values, axis=-1, keepdims=True)]
    all_to_all x1 -> x0, waiting for transfers between devices: 13.5 us -> none  [on_device(): lax.all_to_all(summed.reshape(ep_ranks, slot_count, model_width), 'ep', s...]
  transfers between devices with their start and end apart: 5 -> 0, of which waited for: 5 -> 0; matrix products, arithmetic and copies ran while one was open for 4% -> 0% of each run, Pallas kernels for 0% -> 0%
where the time goes in v1:
time: 118 us
  Pallas kernels  111 us (94%)
  local copies, waits for them, and re-layouts  6.7 us (6%)
    pallas_call x1, Pallas kernels, fused(): pl.pallas_call(functools.partial(fused_kernel, n, slots, reach), out_shap...  111 us
    unnamed x4, local copies, waits for them, and re-layouts  6.7 us

profile of v1, /device:TPU:0, one launch (start us, length us, event | category | flops | bytes accessed | tf_op | source)
XLA Modules:
  0.0 118.0 jit_solution(819625381607481992)
XLA Ops:
  0.6 1.4 %copy.17.weight_ref = f32[128,2]{1,0:T(8,128)} copy(f32[128,2]{0,1:T(2,128)} %param.27) | data formatting | bytes 2048 | tf_op args[13]
  2.0 1.5 %copy.16.index_ref = s32[512,2]{1,0:T(8,128)} copy(s32[512,2]{0,1:T(2,128)} %param.26) | data formatting | bytes 8192 | tf_op args[12]
  3.6 110.6 %shard_map.149 = (bf16[512,512]{1,0:T(8,128)(2,1)}, bf16[128,2048]{1,0:T(8,128)(2,1)}) custom-call(bf16[128,2048]{1,0:T(8,128)(2,1)} %conv_in.1, f32[31,2048]{1,0:T(8,128)} %taps.1, f32[1,2048]{1,0:T(1,128)} %bitcast.2, bf16[2048,512]{1,0:T(8,128)(2,1)} %out_w_hbm.1, bf16[128,2048]{1,0:T(8,128)(2,1)} %moe_in.1, f32[1,2048]{1,0:T(1,128)} %bitcast.3, ...), custom_call_target="tpu_custom_call" | custom-call | tf_op jit(solution)/shard_map/pallas_call | solution.py:483
  114.2 1.9 %copy.20 = bf16[512,512]{1,0:T(8,128)(2,1)} copy(bf16[512,512]{1,0:T(8,128)(2,1)} %get-tuple-element.4) | data formatting | bytes 1048576
  116.1 1.9 %copy.21 = bf16[128,2048]{1,0:T(8,128)(2,1)} copy(bf16[128,2048]{1,0:T(8,128)(2,1)} %get-tuple-element.5) | data formatting | bytes 1048576

commit v2 on v1

--- a/solution.py
+++ b/solution.py
@@ -195,6 +195,7 @@
     after = lax.rem(place + 1, n * 4)
     ahead = lax.rem(place + n * 4 - 1, n * 4)
     halo_rows = halo.shape[0]
+    half = n // 2
 
     fetches = [
         pltpu.make_async_copy(src, dst, local_sem.at[i])
@@ -233,8 +234,12 @@
             device_id_type=MESH,
         )
 
+    def hop(k):
+        odd = lax.rem(k, 2)
+        return odd * (half + k // 2) + (1 - odd) * lax.rem(half - k // 2, half)
+
     def dispatch_copy(k):
-        return remote(own.at[k], gath.at[k, t], 0, k, (lax.rem(e + k, n), t))
+        return remote(own.at[k], gath.at[k, t], 0, k, (lax.rem(e + hop(k), n), t))
 
     def share_core(k, q):
         return remote(gath.at[k, q], gath.at[k, q], 1, k, (e, core_peer))
@@ -252,7 +257,7 @@
         return remote(pair_sum.at[k], from_y.at[k], 6, k, (e, y_peer))
 
     def return_copy(k):
-        return remote(result.at[k], returned.at[k], 7, k, (lax.rem(e - k + n, n), t))
+        return remote(result.at[k], returned.at[k], 7, k, (lax.rem(e - hop(k) + n, n), t))
 
     halo_copy = conv_copy(
         conv_in.at[pl.ds(tokens - halo_rows, halo_rows)],
@@ -269,11 +274,16 @@
 
     lax.fori_loop(0, tokens // ROW_TILE, normal_rows, 0)
 
-    chosen = index_ref[pl.ds(pl.multiple_of(t * tokens, tokens), tokens), :]
+    def column(row_data):
+        return jnp.broadcast_to(row_data, (LANES, tokens)).T[:, 0:1]
+
+    chosen = index_ref[:, pl.ds(pl.multiple_of(t * tokens, tokens), tokens)]
     relative = chosen - e
     relative = jnp.where(relative < 0, relative + n, relative)
-    first, second = relative[:, 0:1], relative[:, 1:2]
-    lane = lax.broadcasted_iota(jnp.int32, (tokens, LANES), 1)
+    order = jnp.where(relative >= half, 2 * (relative - half) + 1, 2 * (half - relative))
+    order = jnp.where(order == n, 0, order).astype(jnp.float32)
+    first, second = column(order[0:1, :]), column(order[1:2, :])
+    lane = lax.broadcasted_iota(jnp.int32, (tokens, LANES), 1).astype(jnp.float32)
     hot_first = (lane == first).astype(jnp.float32)
     hot_second = (lane == second).astype(jnp.float32)
     earlier = (
@@ -283,8 +293,8 @@
     before = jnp.dot(
         earlier, (hot_first + hot_second).astype(jnp.bfloat16), preferred_element_type=jnp.float32
     )
-    slot_first = first.astype(jnp.float32) * slots + jnp.sum(before * hot_first, axis=1, keepdims=True)
-    slot_second = second.astype(jnp.float32) * slots + jnp.sum(
+    slot_first = first * slots + jnp.sum(before * hot_first, axis=1, keepdims=True)
+    slot_second = second * slots + jnp.sum(
         before * hot_second, axis=1, keepdims=True
     )
     row_first = jnp.broadcast_to(slot_first, (tokens, LANES)).T[0:1, :]
@@ -416,8 +426,8 @@
 
     shared = gated(normal[...], sh_gate[...], sh_up[...])
     slot_lane = lax.broadcasted_iota(jnp.int32, (tokens, n * slots), 1).astype(jnp.float32)
-    share = jnp.where(slot_lane == slot_first, weight_ref[:, 0:1], 0.0) + jnp.where(
-        slot_lane == slot_second, weight_ref[:, 1:2], 0.0
+    share = jnp.where(slot_lane == slot_first, column(weight_ref[0:1, :]), 0.0) + jnp.where(
+        slot_lane == slot_second, column(weight_ref[1:2, :]), 0.0
     )
     share_high = share.astype(jnp.bfloat16)
     share_low = (share - share_high.astype(jnp.float32)).astype(jnp.bfloat16)
@@ -528,8 +538,8 @@
         shared_gate,
         shared_up,
         shared_down,
-        expert_index,
-        routing_weight,
+        expert_index.T,
+        routing_weight.T,
     )
 
 
@@ -550,6 +560,7 @@
         and slots % ROW_TILE == 0
         and slots >= ROW_TILE
         and n <= LANES
+        and n % 2 == 0
     )
 
 

time: 118 us -> 112 us (0.949)
  Pallas kernels: 111 us -> 108 us
  local copies, waits for them, and re-layouts: 6.7 us -> 3.75 us
    pallas_call x1, Pallas kernels: 111 us -> 108 us  [fused(): pl.pallas_call(functools.partial(fused_kernel, n, slots, reach), out_shap...]
    unnamed x4 -> x2, local copies, waits for them, and re-layouts: 6.7 us -> 3.75 us
where the time goes in v2:
time: 112 us
  Pallas kernels  108 us (96%)
  local copies, waits for them, and re-layouts  3.75 us (3%)
    pallas_call x1, Pallas kernels, fused(): pl.pallas_call(functools.partial(fused_kernel, n, slots, reach), out_shap...  108 us
    unnamed x2, local copies, waits for them, and re-layouts  3.75 us

profile of v2, /device:TPU:0, one launch (start us, length us, event | category | flops | bytes accessed | tf_op | source)
XLA Modules:
  0.0 111.9 jit_solution(17837914651313746477)
XLA Ops:
  0.6 107.5 %shard_map.149 = (bf16[512,512]{1,0:T(8,128)(2,1)}, bf16[128,2048]{1,0:T(8,128)(2,1)}) custom-call(bf16[128,2048]{1,0:T(8,128)(2,1)} %conv_in.1, f32[31,2048]{1,0:T(8,128)} %taps.1, f32[1,2048]{1,0:T(1,128)} %bitcast.4, bf16[2048,512]{1,0:T(8,128)(2,1)} %out_w_hbm.1, bf16[128,2048]{1,0:T(8,128)(2,1)} %moe_in.1, f32[1,2048]{1,0:T(1,128)} %bitcast.5, ...), custom_call_target="tpu_custom_call" | custom-call | tf_op jit(solution)/shard_map/pallas_call | solution.py:493
  108.2 1.9 %copy.18 = bf16[512,512]{1,0:T(8,128)(2,1)} copy(bf16[512,512]{1,0:T(8,128)(2,1)} %get-tuple-element.4) | data formatting | bytes 1048576
  110.1 1.9 %copy.19 = bf16[128,2048]{1,0:T(8,128)(2,1)} copy(bf16[128,2048]{1,0:T(8,128)(2,1)} %get-tuple-element.5) | data formatting | bytes 1048576
